TPU v7x, 32 devices: a whole 2x2x4 slice. The times are simulated.
32 devices in a mesh: ep: 4 (over z), tp: 8 (over y, x, core).
Axes of the slice: x: 2, y: 2, z: 4, core: 2. Of those that a mesh axis runs over, the one named last changes fastest.
Arguments:
- tokens: bfloat16 [640, 2048], P('ep', 'tp'), may hold values from -6 to 6
- cotangent: bfloat16 [640, 2048], P('ep', 'tp'), may hold values from -6 to 6
- routes: int32 [640, 2], P('ep'), may hold values from 0 to 23, all different within a row; in each aligned block of 160 rows (0 to 159, 160 to 319, ...) at most 14 rows name the same one
- gate_weights: float32 [640, 2], P('ep'), may hold values from 0.2 to 2.5
- expert_gate: bfloat16 [24, 2048, 512], P('ep', 'tp'), may hold values from -0.125 to 0.125
- expert_up: bfloat16 [24, 2048, 512], P('ep', 'tp'), may hold values from -0.125 to 0.125
- expert_down: bfloat16 [24, 512, 2048], P('ep', None, 'tp'), may hold values from -0.25 to 0.25
- shared_gate: bfloat16 [2048, 576], P('tp'), may hold values from -0.125 to 0.125
- shared_up: bfloat16 [2048, 576], P('tp'), may hold values from -0.125 to 0.125
- shared_down: bfloat16 [576, 2048], P(None, 'tp'), may hold values from -0.25 to 0.25
Outputs:
- token_grad: bfloat16 [640, 2048], P('ep', 'tp')
- weight_grad: float32 [640, 2], P('ep')
- expert_gate_grad: float32 [24, 2048, 512], P('ep', 'tp')
- expert_up_grad: float32 [24, 2048, 512], P('ep', 'tp')
- expert_down_grad: float32 [24, 512, 2048], P('ep', None, 'tp')
- shared_gate_grad: float32 [2048, 576], P('tp', 'ep')
- shared_up_grad: float32 [2048, 576], P('tp', 'ep')
- shared_down_grad: float32 [576, 2048], P('ep', 'tp')
- gate_rows_sq: float32 [24, 2048], P('ep', 'tp')
- up_rows_sq: float32 [24, 2048], P('ep', 'tp')
- down_rows_sq: float32 [24, 512], P('ep')
- shared_gate_rows_sq: float32 [2048], P('tp')
- shared_up_rows_sq: float32 [2048], P('tp')
- shared_down_rows_sq: float32 [576], P('ep')
Inputs may be any that keep to these rules, and one draw needn't show every extreme that they name: `routes`: each row names 2 different experts. Among the rows of one index of ep (aligned blocks of 160 rows) no expert is named more than 14 times, a bound that some block reaches.
All inputs are finite; a program needn't handle non-finite values.
Results may differ from a plain program's by a relative error of at most 0.0059.
Values may be sent and summed in bfloat16 or wider, within the bound.
A program may use at most 64 MiB of HBM per device.

v0:
```python
import functools

import jax
import jax.numpy as jnp
from jax import lax
from jax.experimental import pallas as pl
from jax.experimental.pallas import tpu as pltpu
from jax.sharding import PartitionSpec as P

BF = jnp.bfloat16
F32 = jnp.float32
MESH = pl.DeviceIdType.MESH
VMEM = pl.BlockSpec(memory_space=pltpu.VMEM)


def up_to(value, unit):
    return (value + unit - 1) // unit * unit


def silu_parts(pre):
    logistic = jax.nn.sigmoid(pre)
    return (pre * logistic, logistic * (1.0 + pre * (1.0 - logistic)))


def remote(src, dst, send, recv, where):
    return pltpu.make_async_remote_copy(
        src_ref=src,
        dst_ref=dst,
        send_sem=send,
        recv_sem=recv,
        device_id=where,
        device_id_type=MESH,
    )


def greet(places):
    barrier = pltpu.get_barrier_semaphore()
    for place in places:
        pl.semaphore_signal(barrier, inc=1, device_id=place, device_id_type=MESH)
    pl.semaphore_wait(barrier, len(places))


def dot(left, right, left_dim, right_dim, precision=None):
    return lax.dot_general(
        left,
        right,
        (((left_dim,), (right_dim,)), ((), ())),
        precision=precision,
        preferred_element_type=F32,
    )


def front_kernel(
    n_ep, n_tp, experts, per_expert, capacity, picks, cols,
    x, dy, meta, w_gate, w_up, w_down, s_in, s_in_back, s_out_w,
    all_x, all_dy, all_meta, oh, recv_x, weighted, hid, gg, gu, so, dots, token_part,
    wg, wu, wd, rw, g, u, b, s, pg, pu, pb, ps, hg, hu, hb, hs, cg, cu, cb, cs,
    w_sem, z_send, z_recv, a_send, a_recv, b_send, b_recv, c_send, c_recv, d_send, d_recv,
):
    ep, me = lax.axis_index("ep"), lax.axis_index("tp")
    half = n_tp // 2
    parity = lax.rem(me, 2)
    mine = me // 2
    partner = {"tp": me + 1 - 2 * parity}
    others = [lax.rem(mine + d, half) for d in range(1, half)]
    places = [{"tp": 2 * j + parity} for j in others]
    eps = [lax.rem(ep + d, n_ep) for d in range(1, n_ep)]
    tok = x.shape[0]
    rows = g.shape[0] // n_tp
    s_rows = s.shape[0] // n_tp
    used = experts * per_expert
    loads = []
    for k, (src, dst) in enumerate(((w_gate, wg), (w_up, wu), (w_down, wd))):
        loads.append(pltpu.make_async_copy(src, dst, w_sem.at[k]))
        loads[-1].start()
    greet([{"ep": p} for p in eps] + [partner] + places)

    blocks = ((meta, all_meta), (x, all_x), (dy, all_dy))
    gathered = [[], [], []]
    for k, (src, dst) in enumerate(blocks):
        for d, p in enumerate(eps):
            c = remote(src, dst.at[ep], z_send.at[d, k], z_recv.at[d, k], {"ep": p})
            c.start()
            gathered[k].append(c)
    for src, dst in blocks:
        dst[ep] = src[...]
    if used < g.shape[0]:
        oh[...] = jnp.zeros_like(oh)
        rw[...] = jnp.zeros_like(rw)
        for ref in (g, u, b):
            ref[pl.ds(used, g.shape[0] - used), :] = jnp.zeros(
                (g.shape[0] - used, g.shape[1]), F32
            )
    for c in gathered[0]:
        c.wait_recv()
    e_rows = up_to(experts, 8)
    ids = (ep * experts + lax.broadcasted_iota(jnp.int32, (e_rows, tok), 0)).astype(F32)
    before = jnp.where(
        lax.broadcasted_iota(jnp.int32, (tok, tok), 0)
        < lax.broadcasted_iota(jnp.int32, (tok, tok), 1),
        1.0,
        0.0,
    ).astype(BF)
    place_in = lax.broadcasted_iota(jnp.int32, (per_expert, tok), 0).astype(F32)
    sums = [jnp.zeros((per_expert, 1), F32) for _ in range(experts)]
    for blk in range(n_ep):
        info = all_meta[blk]
        chosen = jnp.zeros((e_rows, tok), F32)
        weight_of = jnp.zeros((e_rows, tok), F32)
        for k in range(picks):
            same = info[k : k + 1, :] == ids
            chosen = jnp.where(same, 1.0, chosen)
            weight_of = jnp.where(same, info[picks + k : picks + k + 1, :], weight_of)
        rank = dot(chosen.astype(BF), before, 1, 0)
        slot = jnp.where(chosen > 0.0, rank + float(capacity * blk), -1.0)
        for e in range(experts):
            hot = place_in == slot[e : e + 1, :]
            oh[blk, pl.ds(e * per_expert, per_expert), :] = jnp.where(hot, 1.0, 0.0).astype(BF)
            sums[e] = sums[e] + jnp.sum(
                jnp.where(hot, weight_of[e : e + 1, :], 0.0), axis=1, keepdims=True
            )
    for e in range(experts):
        rw[pl.ds(e * per_expert, per_expert), :] = jnp.broadcast_to(sums[e], (per_expert, 128))

    full = (g, u, b, s)
    got = (pg, pu, pb, ps)
    held = (hg, hu, hb, hs)
    landed = (cg, cu, cb, cs)
    sizes = (rows, rows, rows, s_rows)

    def span(start, size):
        return pl.ds(pl.multiple_of(start * size, size), size)

    first = [None] * 4
    second = [[], [], [], []]

    def swap(k):
        first[k] = remote(
            full[k].at[span(1 - parity, half * sizes[k])],
            got[k],
            a_send.at[k],
            a_recv.at[k],
            partner,
        )
        first[k].start()

    def spread(k):
        first[k].wait()
        held[k][...] = (full[k][span(parity, half * sizes[k]), :] + got[k][...]).astype(BF)
        for d, j in enumerate(others):
            c = remote(
                held[k].at[span(j, sizes[k])],
                landed[k].at[d],
                b_send.at[d, k],
                b_recv.at[d, k],
                places[d],
            )
            c.start()
            second[k].append(c)

    def pick(source):
        total = dot(oh[0], source[0], 1, 0)
        for blk in range(1, n_ep):
            total = total + dot(oh[blk], source[blk], 1, 0)
        return total

    for c in gathered[1]:
        c.wait_recv()
    recv_x[...] = pick(all_x).astype(BF)
    for k, weight in ((0, wg), (1, wu)):
        loads[k].wait()
        for e in range(experts):
            at = pl.ds(e * per_expert, per_expert)
            full[k][at, :] = dot(recv_x[at, :], weight[e], 1, 0)
        swap(k)
    for blk in range(n_ep):
        s[pl.ds(blk * tok, tok), :] = dot(all_x[blk], s_in[...], 1, 1)
    spread(0)
    spread(1)
    for c in gathered[2]:
        c.wait_recv()
    recv_dy = pick(all_dy)
    weighted[...] = (rw[...][:, :1] * recv_dy).astype(BF)
    hid_dy = recv_dy.astype(BF)
    loads[2].wait()
    for e in range(experts):
        b[pl.ds(e * per_expert, per_expert), :] = dot(
            hid_dy[e * per_expert : (e + 1) * per_expert, :], wd[e], 1, 1
        )
    swap(2)
    for blk in range(n_ep):
        s[pl.ds(blk * tok, tok), :] += dot(all_dy[blk], s_in_back[...], 1, 1)
    swap(3)
    spread(2)
    spread(3)

    place = parity * half + mine

    def total(k):
        for c in second[k]:
            c.wait_recv()
        out = full[k][span(place, sizes[k]), :] + got[k][span(mine, sizes[k]), :]
        for d in range(half - 1):
            out = out + landed[k][d].astype(F32)
        return out

    last = []

    def share(k, ref, where):
        block = ref.at[where]
        for d in range(half - 1):
            c = remote(block, block, c_send.at[d, k], c_recv.at[d, k], places[d])
            c.start()
            last.append(c)
        c = remote(block, block, d_send.at[0, k], d_recv.at[0, k], partner)
        c.start()
        last.append(c)

    outs = ((hid, rows), (gg, rows), (gu, rows), (dots, 1), (so, s_rows))

    def part(k, index):
        return pl.ds(index, 1) if k == 3 else span(index, outs[k][1])

    gate, up, back = total(0), total(1), total(2)
    silu_out, silu_slope = silu_parts(gate)
    hidden = (silu_out * up).astype(BF)
    mine_rows = span(place, rows)
    dhidden = rw[mine_rows, :][:, :1] * back
    hid[mine_rows, :] = hidden
    gg[mine_rows, :] = (dhidden * up * silu_slope).astype(BF)
    gu[mine_rows, :] = (dhidden * silu_out).astype(BF)
    dots[place] = dot(
        jnp.ones((8, gate.shape[1]), F32),
        hidden.astype(F32) * back,
        1,
        1,
        lax.Precision.HIGHEST,
    )
    for k in range(4):
        share(k, outs[k][0], part(k, place))

    both = total(3)
    width = both.shape[1]
    lane = lax.broadcasted_iota(jnp.int32, both.shape, 1)
    s_up = pltpu.roll(both, width - cols, 1)
    s_back = pltpu.roll(both, width - 2 * cols, 1)
    s_out, s_slope = silu_parts(both)
    s_dgate = pltpu.roll(s_back * s_up * s_slope, cols, 1)
    s_dup = pltpu.roll(s_back * s_out, 2 * cols, 1)
    so[span(place, s_rows), :] = jnp.where(
        lane < cols, s_out * s_up, jnp.where(lane < 2 * cols, s_dgate, s_dup)
    ).astype(BF)
    share(4, so, part(4, place))

    def forward(k):
        ref = outs[k][0]
        for d in range(half - 1):
            source = lax.rem(mine + half - 1 - d, half)
            block = ref.at[part(k, parity * half + source)]
            remote(
                block, block, c_send.at[d, k], c_recv.at[d, k], places[d]
            ).wait_recv()
            c = remote(block, block, d_send.at[1 + d, k], d_recv.at[1 + d, k], partner)
            c.start()
            last.append(c)

    def settle(k):
        ref = outs[k][0]
        for d in range(half):
            source = mine if d == 0 else lax.rem(mine + half - d, half)
            block = ref.at[part(k, (1 - parity) * half + source)]
            remote(block, block, d_send.at[d, k], d_recv.at[d, k], partner).wait_recv()

    for k in range(4):
        forward(k)
    for k in range(4):
        settle(k)
    row_grad = []
    for e in range(experts):
        at = pl.ds(e * per_expert, per_expert)
        row_grad.append(
            (dot(gg[at, :], wg[e], 1, 1) + dot(gu[at, :], wu[e], 1, 1)).astype(BF)
        )
    if used < g.shape[0]:
        row_grad.append(jnp.zeros((g.shape[0] - used, x.shape[1]), BF))
    row_grad = jnp.concatenate(row_grad, axis=0)
    forward(4)
    settle(4)
    for blk in range(n_ep):
        token_part[blk] = (
            dot(oh[blk], row_grad, 0, 0)
            + dot(so[pl.ds(blk * tok, tok), :], s_out_w[...], 1, 0)
        ).astype(BF)
    for group in second:
        for c in group:
            c.wait_send()
    for group in gathered:
        for c in group:
            c.wait_send()
    for c in last:
        c.wait_send()


def row_squares(square):
    ones = jnp.ones((8, square.shape[1]), BF)
    high = square.astype(BF)
    low = (square - high.astype(F32)).astype(BF)
    return (dot(ones, high, 1, 1) + dot(ones, low, 1, 1))[:1, :]


def weights_kernel(
    experts, cols,
    recv_x, weighted, hid, gg, gu, all_x, all_dy, so,
    gate_out, up_out, down_out, sg_out, su_out, sd_out, gate_sq, up_sq, over_tp, over_ep,
):
    e = pl.program_id(0)
    gate = dot(recv_x[...], gg[...], 0, 0)
    gate_out[0] = gate
    gate_sq[pl.ds(e, 1), :] = row_squares(gate * gate)
    up = dot(recv_x[...], gu[...], 0, 0)
    up_out[0] = up
    up_sq[pl.ds(e, 1), :] = row_squares(up * up)
    down = dot(hid[...], weighted[...], 0, 0)
    down_out[0] = down

    @pl.when(e == 0)
    def _():
        over_tp[...] = jnp.zeros_like(over_tp)
        over_ep[...] = jnp.zeros_like(over_ep)
        pair = dot(so[...], all_x[...], 0, 0)
        sg, su = pair[cols : 2 * cols, :], pair[2 * cols : 3 * cols, :]
        sg_out[...] = sg
        su_out[...] = su
        over_ep[0:1, :] = jnp.sum(sg * sg, axis=0, keepdims=True)
        over_ep[1:2, :] = jnp.sum(su * su, axis=0, keepdims=True)
        sd_full = dot(so[...], all_dy[...], 0, 0)
        sd_out[...] = sd_full[:cols, :]
        sq = row_squares(sd_full * sd_full)
        kept = lax.broadcasted_iota(jnp.int32, sq.shape, 1) < cols
        sq = jnp.where(kept, sq, 0.0)
        span = min(over_tp.shape[1], sq.shape[1])
        over_tp[experts : experts + 1, :span] = sq[:, :span]

    over_tp[pl.ds(e, 1), :] = row_squares(down * down)


def finish_kernel(
    n_ep, n_tp, wg, es, ts, wg_out, es_out, ts_out,
    wg_in, es_in, ts_in, e_send, e_recv, t_send, t_recv,
):
    ep, tp = lax.axis_index("ep"), lax.axis_index("tp")
    eps = [lax.rem(ep + d, n_ep) for d in range(1, n_ep)]
    tps = [lax.rem(tp + d, n_tp) for d in range(1, n_tp)]
    greet([{"ep": p} for p in eps] + [{"tp": p} for p in tps])
    copies = []
    for d, p in enumerate(eps):
        for k, (src, dst) in enumerate(((wg.at[p], wg_in.at[d]), (es, es_in.at[d]))):
            copies.append(remote(src, dst, e_send.at[d, k], e_recv.at[d, k], {"ep": p}))
            copies[-1].start()
    for d, p in enumerate(tps):
        copies.append(remote(ts, ts_in.at[d], t_send.at[d], t_recv.at[d], {"tp": p}))
        copies[-1].start()
    for c in copies:
        c.wait()
    weights = wg[ep]
    norms = es[...]
    for d in range(n_ep - 1):
        weights = weights + wg_in[d]
        norms = norms + es_in[d]
    wg_out[...] = weights
    es_out[...] = norms
    down = ts[...]
    for d in range(n_tp - 1):
        down = down + ts_in[d]
    ts_out[...] = down


def call(kernel, collective, outs, scratch, *args, specs=None):
    return pl.pallas_call(
        kernel,
        out_shape=[jax.ShapeDtypeStruct(s, t) for s, t in outs],
        in_specs=specs or [VMEM] * len(args),
        out_specs=[VMEM] * len(outs),
        scratch_shapes=scratch,
        compiler_params=pltpu.CompilerParams(
            collective_id=collective,
            has_side_effects=True,
            vmem_limit_bytes=48 * 1024 * 1024,
        ),
    )(*args)


def per_device(
    n_ep, n_tp,
    tokens, cotangent, routes, gate_weights,
    expert_gate, expert_up, expert_down,
    shared_gate, shared_up, shared_down,
):
    dma = pltpu.SemaphoreType.DMA
    half = n_tp // 2
    tok_rows, narrow = tokens.shape
    picks = routes.shape[1]
    experts, _, ff = expert_gate.shape
    experts_all = experts * n_ep
    capacity = max(2, (tok_rows * picks + experts_all - 1) // experts_all)
    every = tok_rows * n_ep
    cols = shared_gate.shape[1] // n_ep
    ep = lax.axis_index("ep")
    per_expert = up_to(capacity * n_ep, 16)
    used = experts * per_expert
    rows = up_to(used, 16 * n_tp)
    width = up_to(3 * cols, 128)
    chunk, s_chunk = rows // n_tp, every // n_tp

    meta = jnp.concatenate([routes.astype(F32).T, gate_weights.T], axis=0)
    meta = jnp.pad(meta, ((0, up_to(2 * picks, 8) - 2 * picks), (0, 0)))
    sg = lax.dynamic_slice_in_dim(shared_gate.T, ep * cols, cols, 0)
    su = lax.dynamic_slice_in_dim(shared_up.T, ep * cols, cols, 0)
    sd = lax.dynamic_slice_in_dim(shared_down, ep * cols, cols, 0)
    s_in = jnp.pad(jnp.concatenate([sg, su], axis=0), ((0, width - 2 * cols), (0, 0)))
    s_in_back = jnp.pad(sd, ((2 * cols, width - 3 * cols), (0, 0)))
    s_out_w = jnp.pad(jnp.concatenate([sg, su], axis=0), ((cols, width - 3 * cols), (0, 0)))
    anywhere = pl.BlockSpec(memory_space=pl.ANY)
    vm = pltpu.VMEM
    (
        all_x, all_dy, all_meta, onehot, recv_x, weighted,
        hidden, grad_gate, grad_up, s_all, dots, token_part,
    ) = call(
        functools.partial(
            front_kernel, n_ep, n_tp, experts, per_expert, capacity, picks, cols
        ),
        0,
        [
            ((n_ep, tok_rows, narrow), BF),
            ((n_ep, tok_rows, narrow), BF),
            ((n_ep,) + meta.shape, F32),
            ((n_ep, rows, tok_rows), BF),
            ((rows, narrow), BF),
            ((rows, narrow), BF),
            ((rows, ff), BF),
            ((rows, ff), BF),
            ((rows, ff), BF),
            ((every, width), BF),
            ((n_tp, 8, chunk), F32),
            ((n_ep, tok_rows, narrow), BF),
        ],
        [
            vm(expert_gate.shape, BF), vm(expert_up.shape, BF), vm(expert_down.shape, BF),
            vm((rows, 128), F32),
        ]
        + [vm((rows, ff), F32)] * 3 + [vm((every, width), F32)]
        + [vm((rows // 2, ff), F32)] * 3 + [vm((every // 2, width), F32)]
        + [vm((rows // 2, ff), BF)] * 3 + [vm((every // 2, width), BF)]
        + [vm((half - 1, chunk, ff), BF)] * 3 + [vm((half - 1, s_chunk, width), BF)]
        + [
            dma((3,)), dma((n_ep - 1, 3)), dma((n_ep - 1, 3)),
            dma((4,)), dma((4,)), dma((half - 1, 4)), dma((half - 1, 4)),
            dma((half - 1, 5)), dma((half - 1, 5)), dma((half, 5)), dma((half, 5)),
        ],
        tokens, cotangent, meta, expert_gate, expert_up, expert_down,
        s_in, s_in_back, s_out_w,
        specs=[VMEM] * 3 + [anywhere] * 3 + [VMEM] * 3,
    )
    token_grad = token_part[ep].astype(F32)
    for d in range(1, n_ep):
        moved = lax.ppermute(
            lax.dynamic_index_in_dim(token_part, lax.rem(ep + d, n_ep), 0, False),
            "ep",
            [(i, (i + d) % n_ep) for i in range(n_ep)],
        )
        token_grad = token_grad + moved.astype(F32)
    token_grad = token_grad.astype(BF)

    whole_x = all_x.reshape(every, narrow)
    whole_dy = all_dy.reshape(every, narrow)
    norm_rows = up_to(experts + 1, 8)

    def fixed(shape):
        return pl.BlockSpec(shape, lambda e: (0,) * len(shape))

    def rowed(columns):
        return pl.BlockSpec((per_expert, columns), lambda e: (e, 0))

    def stacked(a, c):
        return pl.BlockSpec((1, a, c), lambda e: (e, 0, 0))

    flops = 2 * experts * per_expert * narrow * ff * 3 + 4 * every * narrow * width
    (
        gate_wgrad, up_wgrad, down_grad, sg_grad, su_grad, sd_grad,
        gate_rows_sq, up_rows_sq, over_tp, over_ep,
    ) = pl.pallas_call(
        functools.partial(weights_kernel, experts, cols),
        grid=(experts,),
        in_specs=[rowed(narrow), rowed(narrow), rowed(ff), rowed(ff), rowed(ff)]
        + [fixed(whole_x.shape), fixed(whole_dy.shape), fixed(s_all.shape)],
        out_specs=[stacked(narrow, ff), stacked(narrow, ff), stacked(ff, narrow)]
        + [fixed((cols, narrow))] * 3
        + [fixed((experts, narrow))] * 2
        + [fixed((norm_rows, ff)), fixed((8, narrow))],
        out_shape=[
            jax.ShapeDtypeStruct(shape, F32)
            for shape in (
                (experts, narrow, ff), (experts, narrow, ff), (experts, ff, narrow),
                (cols, narrow), (cols, narrow), (cols, narrow),
                (experts, narrow), (experts, narrow), (norm_rows, ff), (8, narrow),
            )
        ],
        cost_estimate=pl.CostEstimate(
            flops=flops, bytes_accessed=experts * narrow * ff * 12, transcendentals=0
        ),
        compiler_params=pltpu.CompilerParams(
            dimension_semantics=("arbitrary",), vmem_limit_bytes=48 * 1024 * 1024
        ),
    )(recv_x, weighted, hidden, grad_gate, grad_up, whole_x, whole_dy, s_all)

    ids = (ep * experts + jnp.arange(experts, dtype=jnp.int32)).astype(F32)
    match = all_meta[:, :picks, None, :] == ids[None, None, :, None]
    hot = onehot[:, :used].reshape(n_ep, experts, per_expert, tok_rows)
    row_dots = dots[:, 0, :].reshape(rows)[:used].reshape(1, experts, per_expert, 1)
    dot_of = jnp.sum(hot.astype(F32) * row_dots, axis=2)
    weight_part = jnp.sum(jnp.where(match, dot_of[:, None], 0.0), axis=2)
    weight_part = jnp.pad(weight_part, ((0, 0), (0, up_to(picks, 8) - picks), (0, 0)))
    peers, t_peers = n_ep - 1, n_tp - 1
    weight_grad, over_ep, over_tp = call(
        functools.partial(finish_kernel, n_ep, n_tp),
        1,
        [(weight_part.shape[1:], F32), (over_ep.shape, F32), (over_tp.shape, F32)],
        [
            vm((peers,) + weight_part.shape[1:], F32),
            vm((peers,) + over_ep.shape, F32),
            vm((t_peers,) + over_tp.shape, F32),
            dma((peers, 2)), dma((peers, 2)), dma((t_peers,)), dma((t_peers,)),
        ],
        weight_part, over_ep, over_tp,
    )
    return (
        token_grad,
        weight_grad[:picks].T,
        gate_wgrad,
        up_wgrad,
        down_grad,
        sg_grad.T,
        su_grad.T,
        sd_grad,
        gate_rows_sq,
        up_rows_sq,
        over_tp[:experts],
        over_ep[0],
        over_ep[1],
        over_tp[experts, :cols],
    )


def solution(mesh):
    n_ep, n_tp = mesh.shape["ep"], mesh.shape["tp"]
    return jax.shard_map(
        functools.partial(per_device, n_ep, n_tp),
        mesh=mesh,
        in_specs=(
            P("ep", "tp"),
            P("ep", "tp"),
            P("ep", None),
            P("ep", None),
            P("ep", "tp", None),
            P("ep", "tp", None),
            P("ep", None, "tp"),
            P("tp", None),
            P("tp", None),
            P(None, "tp"),
        ),
        out_specs=(
            P("ep", "tp"),
            P("ep", None),
            P("ep", "tp", None),
            P("ep", "tp", None),
            P("ep", None, "tp"),
            P("tp", "ep"),
            P("tp", "ep"),
            P("ep", "tp"),
            P("ep", "tp"),
            P("ep", "tp"),
            P("ep", None),
            P("tp"),
            P("tp"),
            P("ep"),
        ),
        check_vma=False,
    )
```

profile of v0, /device:TPU:0, one launch (start us, length us, event | category | flops | bytes accessed | tf_op | source)
XLA Modules:
  0.0 79.3 jit_solution(791651854833213691)
XLA Ops:
  0.6 0.0 copy-start
  0.7 0.0 copy-start.10
  0.7 0.7 convert_bitcast_fusion
  1.4 0.2 copy-done
  1.6 0.9 %dynamic-slice_bitcast_fusion.3 = (bf16[144,256]{1,0:T(8,128)(2,1)S(1)}, bf16[144,256]{1,0:T(8,128)(2,1)S(1)}) fusion(bf16[256,576]{0,1:T(8,128)(2,1)} %param.18, s32[]{:T(128)S(6)} %select_n.22, bf16[256,576]{0,1:T(8,128)(2,1)} %param.17), kind=kLoop, calls=%fused_computation.10 | loop fusion | bytes 294916 | tf_op jit(solution)/shard_map/dynamic_slice | solution.py:418
  2.6 0.7 select_maximum_fusion.meta
  3.4 0.0 copy-done.10
  3.4 0.0 copy-start.11
  3.4 0.9 %copy-done.11 = bf16[160,256]{1,0:T(8,128)(2,1)S(1)} copy-done((bf16[160,256]{1,0:T(8,128)(2,1)S(1)}, bf16[160,256]{1,0:T(8,128)(2,1)}, u32[]{:S(2)}) %copy-start.11) | copy-done | bytes 81944
  4.3 44.8 %shard_map.209 = (bf16[4,160,256]{2,1,0:T(8,128)(2,1)S(1)}, bf16[4,160,256]{2,1,0:T(8,128)(2,1)S(1)}, f32[4,8,160]{2,1,0:T(8,128)S(1)}, bf16[4,384,160]{2,1,0:T(...) custom-call(bf16[160,256]{1,0:T(8,128)(2,1)S(1)} %copy-done.10, ...), custom_call_target="tpu_custom_call" | custom-call | tf_op jit(solution)/shard_map/pallas_call | solution.py:379
  49.1 0.0 copy-start.4
  49.1 0.7 copy-done.4
  49.8 0.0 copy-start.6
  49.8 0.7 copy-done.6
  50.5 0.0 copy-start.8
  50.5 0.7 copy-done.8
  51.2 0.0 copy-start.1
  51.2 0.0 copy-start.2
  51.2 0.0 copy-start.12
  51.2 0.7 copy-done.1
  51.9 0.0 copy-start.5
  51.9 0.7 dynamic-slice_bitcast_fusion.2
  52.6 0.0 copy-done.2
  52.6 0.0 copy-done.12
  52.6 2.5 %collective-permute-start = (bf16[160,256]{1,0:T(8,128)(2,1)}, bf16[160,256]{1,0:T(8,128)(2,1)}, u32[]{:S(2)}, u32[]{:S(2)}) collective-permute-start(bf16[160,256]{1,0:T(8,128)(2,1)} %get-tuple-element.64), channel_id=1, source_target_pairs={{0,8},{8,16},{16,24},{24,0},{1,9},{9,17},{17,25},{25,1},{2,10},{10... | collective-permute-start | bytes 245768 | tf_op jit(solution)/shard_map/ppermute | solution.py:466
  55.1 1.3 %collective-permute-start.2 = (bf16[160,256]{1,0:T(8,128)(2,1)}, bf16[160,256]{1,0:T(8,128)(2,1)}, u32[]{:S(2)}, u32[]{:S(2)}) collective-permute-start(bf16[160,256]{1,0:T(8,128)(2,1)} %get-tuple-element.65), channel_id=1, source_target_pairs={{0,24},{8,0},{16,8},{24,16},{1,25},{9,1},{17,9},{25,17},{2,26},{10... | collective-permute-start | bytes 245768 | tf_op jit(solution)/shard_map/ppermute | solution.py:466
  56.4 0.3 collective-permute-start.1
  56.7 0.5 add_convert_fusion
  57.3 0.8 slice_reduce_fusion
  58.0 0.1 mul.20
  58.1 0.3 fusion
  58.5 0.7 select_reduce_fusion
  59.2 0.0 copy-done.5
  59.2 0.0 copy-done.7
  59.2 0.0 copy-start.3
  59.3 1.0 %copy-done.3 = bf16[4,160,256]{2,1,0:T(8,128)(2,1)S(1)} copy-done((bf16[4,160,256]{2,1,0:T(8,128)(2,1)S(1)}, bf16[4,160,256]{2,1,0:T(8,128)(2,1)}, u32[]{:S(2)}) %copy-start.3) | copy-done | bytes 327704
  60.2 0.0 copy-start.9
  60.2 0.9 %copy-done.9 = bf16[384,256]{1,0:T(8,128)(2,1)S(1)} copy-done((bf16[384,256]{1,0:T(8,128)(2,1)S(1)}, bf16[384,256]{1,0:T(8,128)(2,1)}, u32[]{:S(2)}) %copy-start.9) | copy-done | bytes 196632
  61.2 7.7 %shard_map.210 = (f32[6,256,512]{2,1,0:T(8,128)}, f32[6,256,512]{2,1,0:T(8,128)}, f32[6,512,256]{2,1,0:T(8,128)}, f32[144,256]{1,0:T(8,128)}, f32[144,256]{1,0:T...) custom-call(bf16[384,256]{1,0:T(8,128)(2,1)S(1)} %copy-done.7, ...), custom_call_target="tpu_custom_call" | custom-call | flops 637534208 | bytes 9437184 | tf_op jit(solution)/shard_map/pallas_call | solution.py:491
  68.9 6.4 %shard_map.211 = (f32[8,160]{1,0:T(8,128)S(1)}, f32[8,256]{1,0:T(8,128)S(1)}, f32[8,512]{1,0:T(8,128)S(1)}) custom-call(f32[4,8,160]{2,1,0:T(8,128)S(1)} %pad.24.wg, f32[8,256]{1,0:T(8,128)S(1)} %get-tuple-element.51.es, f32[8,512]{1,0:T(8,128)S(1)} %get-tuple-element.52.ts), custom_call_target="tpu_custom_call" | custom-call | tf_op jit(solution)/shard_map/pallas_call | solution.py:379
  75.3 0.6 slice_bitcast_fusion
  75.9 0.6 fusion.5
  76.4 0.6 slice.27
  77.0 0.0 collective-permute-done
  77.0 0.0 collective-permute-done.2
  77.0 0.0 collective-permute-done.1
  77.0 1.7 %fusion.3 = bf16[160,256]{1,0:T(8,128)(2,1)} fusion(bf16[160,256]{1,0:T(8,128)(2,1)} %collective-permute-done.2, bf16[160,256]{1,0:T(8,128)(2,1)} %collective-permute-done.1, bf16[160,256]{1,0:T(8,128)(2,1)} %collective-permute-done, bf16[4,160,256]{2,1,0:T(8,128)(2,1)} %copy-done.1, s32[]{:T(128)S(6)} %select_n.23), kind=kLoop, calls=%fused_computation.5 | loop fusion | flops 327680 | bytes 409604 | tf_op jit(solution)/shard_map/convert_element_type | solution.py:472
  78.7 0.6 copy.30
  (10 shorter events, 0.1 us)
Async XLA Ops:
  0.6 1.0 %copy-start = (bf16[576,256]{1,0:T(8,128)(2,1)S(1)}, bf16[576,256]{1,0:T(8,128)(2,1)}, u32[]{:S(2)}) copy-start(bf16[576,256]{1,0:T(8,128)(2,1)} %param.19) | copy-start | bytes 884740
  0.7 2.7 %copy-start.10 = (bf16[160,256]{1,0:T(8,128)(2,1)S(1)}, bf16[160,256]{1,0:T(8,128)(2,1)}, u32[]{:S(2)}) copy-start(bf16[160,256]{1,0:T(8,128)(2,1)} %x.11) | copy-start | bytes 245764
  3.4 0.9 %copy-start.11 = (bf16[160,256]{1,0:T(8,128)(2,1)S(1)}, bf16[160,256]{1,0:T(8,128)(2,1)}, u32[]{:S(2)}) copy-start(bf16[160,256]{1,0:T(8,128)(2,1)} %dy.1) | copy-start | bytes 245764
  49.1 0.7 copy-start.4
  49.8 0.7 copy-start.6
  50.5 0.7 copy-start.8
  51.2 0.7 copy-start.1
  51.2 1.4 %copy-start.2 = (bf16[4,160,256]{2,1,0:T(8,128)(2,1)}, bf16[4,160,256]{2,1,0:T(8,128)(2,1)S(1)}, u32[]{:S(2)}) copy-start(bf16[4,160,256]{2,1,0:T(8,128)(2,1)S(1)} %get-tuple-element.48) | copy-start | bytes 983044
  51.2 1.4 %copy-start.12 = (f32[8,8,48]{2,1,0:T(8,128)}, f32[8,8,48]{2,1,0:T(8,128)S(1)}, u32[]{:S(2)}) copy-start(f32[8,8,48]{2,1,0:T(8,128)S(1)} %get-tuple-element.42) | copy-start | bytes 36868
  51.9 7.3 %copy-start.5 = (bf16[4,160,256]{2,1,0:T(8,128)(2,1)S(1)}, bf16[4,160,256]{2,1,0:T(8,128)(2,1)}, u32[]{:S(2)}) copy-start(bf16[4,160,256]{2,1,0:T(8,128)(2,1)} %copy-done.4) | copy-start | bytes 983044
  51.9 7.4 %copy-start.7 = (bf16[384,256]{1,0:T(8,128)(2,1)S(1)}, bf16[384,256]{1,0:T(8,128)(2,1)}, u32[]{:S(2)}) copy-start(bf16[384,256]{1,0:T(8,128)(2,1)} %copy-done.6) | copy-start | bytes 589828
  52.6 24.4 %collective-permute-start = (bf16[160,256]{1,0:T(8,128)(2,1)}, bf16[160,256]{1,0:T(8,128)(2,1)}, u32[]{:S(2)}, u32[]{:S(2)}) collective-permute-start(bf16[160,256]{1,0:T(8,128)(2,1)} %get-tuple-element.64), channel_id=1, source_target_pairs={{0,8},{8,16},{16,24},{24,0},{1,9},{9,17},{17,25},{25,1},{2,10},{10... | collective-permute-start | bytes 245768 | tf_op jit(solution)/shard_map/ppermute | solution.py:466
  55.1 21.9 %collective-permute-start.2 = (bf16[160,256]{1,0:T(8,128)(2,1)}, bf16[160,256]{1,0:T(8,128)(2,1)}, u32[]{:S(2)}, u32[]{:S(2)}) collective-permute-start(bf16[160,256]{1,0:T(8,128)(2,1)} %get-tuple-element.65), channel_id=1, source_target_pairs={{0,24},{8,0},{16,8},{24,16},{1,25},{9,1},{17,9},{25,17},{2,26},{10... | collective-permute-start | bytes 245768 | tf_op jit(solution)/shard_map/ppermute | solution.py:466
  56.4 20.6 %collective-permute-start.1 = (bf16[160,256]{1,0:T(8,128)(2,1)S(1)}, bf16[160,256]{1,0:T(8,128)(2,1)}, u32[]{:S(2)}, u32[]{:S(2)}) collective-permute-start(bf16[160,256]{1,0:T(8,128)(2,1)S(1)} %get-tuple-element.66), channel_id=1, source_target_pairs={{0,16},{8,24},{16,0},{24,8},{1,17},{9,25},{17,1},{25,9},{2,18},{10... | collective-permute-start | bytes 245768 | tf_op jit(solution)/shard_map/ppermute | solution.py:466
  59.2 1.0 %copy-start.3 = (bf16[4,160,256]{2,1,0:T(8,128)(2,1)S(1)}, bf16[4,160,256]{2,1,0:T(8,128)(2,1)}, u32[]{:S(2)}) copy-start(bf16[4,160,256]{2,1,0:T(8,128)(2,1)} %copy-done.2) | copy-start | bytes 983044
  60.2 0.9 %copy-start.9 = (bf16[384,256]{1,0:T(8,128)(2,1)S(1)}, bf16[384,256]{1,0:T(8,128)(2,1)}, u32[]{:S(2)}) copy-start(bf16[384,256]{1,0:T(8,128)(2,1)} %copy-done.8) | copy-start | bytes 589828
where the time goes:
time: 79.7 us; the launch traced here: 79.3 us
  Pallas kernels  58.9 us (74%)
  local copies, waits for them, and re-layouts  10.7 us (13%)
  other arithmetic  4.69 us (6%)
  starting transfers between devices  4.17 us (5%)
  between operations  0.84 us (1%)
    pallas_call x2, Pallas kernels, call(): pl.pallas_call(kernel, out_shape=[jax.ShapeDtypeStruct(s, t) for s, t in...  51.2 us
    pallas_call x1, Pallas kernels, per_device(): pl.pallas_call(functools.partial(weights_kernel, experts, cols), grid=(ex...  7.7 us
    unnamed x27, local copies, waits for them, and re-layouts  6.41 us
    ppermute x3, starting transfers between devices, per_device(): lax.ppermute(lax.dynamic_index_in_dim(token_part, lax.rem(ep + d, n_ep),...  4.17 us
    convert_element_type x1, other arithmetic, per_device(): token_grad = token_grad.astype(BF)  1.69 us
  transfers between devices with their start and end apart: 3, of which 0 were waited for; matrix products, arithmetic and copies ran while one was open for 5% of the time, Pallas kernels for 18%

commit v1 on v0

v1 whole, which is shorter than its diff:
```python
import functools

import jax
import jax.numpy as jnp
from jax import lax
from jax.experimental import pallas as pl
from jax.experimental.pallas import tpu as pltpu
from jax.sharding import PartitionSpec as P

BF = jnp.bfloat16
F32 = jnp.float32
MESH = pl.DeviceIdType.MESH
VMEM = pl.BlockSpec(memory_space=pltpu.VMEM)
HBM = pl.BlockSpec(memory_space=pltpu.HBM)
LANES = 128
WAVE_ROWS = 16
VMEM_BYTES = 67_043_328
ROOM = 14 * 2**20


def up_to(value, unit):
    return (value + unit - 1) // unit * unit


def silu_parts(pre):
    logistic = jax.nn.sigmoid(pre)
    return (pre * logistic, logistic * (1.0 + pre * (1.0 - logistic)))


def remote(src, dst, send, recv, where):
    return pltpu.make_async_remote_copy(
        src_ref=src,
        dst_ref=dst,
        send_sem=send,
        recv_sem=recv,
        device_id=where,
        device_id_type=MESH,
    )


def dot(left, right, left_dim, right_dim, precision=None):
    return lax.dot_general(
        left,
        right,
        (((left_dim,), (right_dim,)), ((), ())),
        precision=precision,
        preferred_element_type=F32,
    )


def row_squares(square):
    ones = jnp.ones((8, square.shape[1]), BF)
    high = square.astype(BF)
    low = (square - high.astype(F32)).astype(BF)
    return (dot(ones, high, 1, 1) + dot(ones, low, 1, 1))[:1, :]


def join(parts, axis):
    return parts[0] if len(parts) == 1 else jnp.concatenate(parts, axis=axis)


def nearest(ep, n_ep, k):
    if k == 0:
        return ep
    left, right = ep, n_ep - 1 - ep
    both = jnp.minimum(left, right)
    paired = jnp.where(2 * both >= k, 1, 0)
    far = jnp.where(paired == 1, (k + 1) // 2, k - both)
    go_left = jnp.where(paired == 1, k % 2, jnp.where(left > right, 1, 0))
    return ep + far * (1 - 2 * go_left)


class Plan:
    def __init__(self, n_ep, n_tp, tok, picks, narrow, experts, ff, shared):
        self.n_ep, self.n_tp, self.tok, self.picks = n_ep, n_tp, tok, picks
        self.narrow, self.experts, self.ff = narrow, experts, ff
        all_experts = experts * n_ep
        self.capacity = max(2, (tok * picks + all_experts - 1) // all_experts)
        self.half = n_tp // 2
        self.nc = ff // LANES
        self.nr = self.half // self.nc
        self.bpw = max(
            b for b in range(1, n_ep + 1)
            if n_ep % b == 0 and (b == 1 or b * self.capacity <= WAVE_ROWS)
        )
        self.waves = n_ep // self.bpw
        self.slots = up_to(self.capacity * self.bpw, 16)
        self.rows = up_to(experts * self.slots, self.slots * 2 * self.nr)
        self.rc = self.rows // (2 * self.nr)
        self.wave_tok = self.bpw * tok
        self.sc = self.wave_tok // (2 * self.nr)
        self.cols = shared // n_ep
        self.cpc = -(-self.cols // self.nc)
        self.slab = 3 * self.rc + self.sc
        self.out_slab = self.slab + 16
        self.e_rows = up_to(experts, 8)
        assert self.half % self.nc == 0 and self.nr > 0 and self.rc <= LANES
        assert self.sc % 16 == 0 and 3 * self.cpc <= LANES

    def place(self, q, c):
        return (q // self.nr) * self.half + (q % self.nr) * self.nc + c

    def strip(self, index):
        row = index * self.slots
        return row // self.rc, row % self.rc


def main_kernel(
    p,
    x, dy, routes, weights, w_gate, w_up, w_down, sg_w, su_w, sd_w,
    token_out, weight_out, gate_out, up_out, down_out, sg_out, su_out, sd_out,
    gate_sq, up_sq, down_sq, sg_sq, su_sq, sd_sq,
    wg, wu, wd, sgv, suv, sdv, rts, gws, all_x, all_dy, all_meta,
    s_in, s_back, s_out_w, oh, recv_x, weighted, rw,
    full, got, held, landed, acts, pair, part, part_in, own, wpart, wpart_in,
    ts, ts_in, es, es_in,
    ld, zo, zs, zr, a_s, a_r, b_s, b_r, c_s, c_r, d_s, d_r, r_s, r_r, e_s, e_r, t_s, t_r,
):
    n_ep, n_tp, half, nc, nr = p.n_ep, p.n_tp, p.half, p.nc, p.nr
    ep, me = lax.axis_index("ep"), lax.axis_index("tp")
    parity = lax.rem(me, 2)
    mine = me // 2
    partner = {"tp": me + 1 - 2 * parity}
    others = [lax.rem(mine + d, half) for d in range(1, half)]
    places = [{"tp": 2 * j + parity} for j in others]
    eps = [lax.rem(ep + d, n_ep) for d in range(1, n_ep)]
    tps = [lax.rem(me + d, n_tp) for d in range(1, n_tp)]
    order = [nearest(ep, n_ep, k) for k in range(n_ep)]
    place = parity * half + mine

    barrier = pltpu.get_barrier_semaphore()
    for where in [{"ep": q} for q in eps] + [{"tp": q} for q in tps]:
        pl.semaphore_signal(barrier, inc=1, device_id=where, device_id_type=MESH)

    span = pl.ds(pl.multiple_of(ep * p.cols, 8), p.cols)
    sources = (
        (x, all_x.at[ep]), (dy, all_dy.at[ep]), (routes, rts), (weights, gws),
        (sg_w.at[span], sgv), (su_w.at[span], suv), (sd_w.at[span], sdv),
        (w_gate, wg), (w_up, wu), (w_down, wd),
    )
    loads = []
    for k, (src, dst) in enumerate(sources):
        loads.append(pltpu.make_async_copy(src, dst, ld.at[k]))
        loads[-1].start()

    loads[2].wait()
    loads[3].wait()
    all_meta[ep] = jnp.concatenate(
        [rts[...].astype(F32), gws[...]]
        + [jnp.zeros((all_meta.shape[1] - 2 * p.picks, p.tok), F32)] * (
            all_meta.shape[1] > 2 * p.picks
        ),
        axis=0,
    )
    loads[0].wait()
    loads[1].wait()
    pl.semaphore_wait(barrier, n_ep + n_tp - 2)

    blocks = (all_meta, all_x, all_dy)

    def relay(b, k, send, step):
        return remote(
            blocks[k].at[b], blocks[k].at[b], send, zr.at[b, k], {"ep": ep + step}
        )

    go_right, go_left = ep < n_ep - 1, ep > 0
    for cond, side, step in ((go_right, 0, 1), (go_left, 1, -1)):

        @pl.when(cond)
        def _(side=side, step=step):
            for k in range(3):
                relay(ep, k, zo.at[side, k], step).start()

    def arrive(k):
        b = order[k]
        if k == 0:
            return
        for a in range(3):
            relay(b, a, zs.at[b, a], 0).wait_recv()

            @pl.when((b < ep) & go_right)
            def _():
                relay(b, a, zs.at[b, a], 1).start()

            @pl.when((b > ep) & go_left)
            def _():
                relay(b, a, zs.at[b, a], -1).start()

    lane_n = lax.broadcasted_iota(jnp.int32, (p.cols, nc * LANES), 1)
    row_i = lax.broadcasted_iota(jnp.int32, (p.cols, nc * LANES), 0)
    chunk = lax.shift_right_logical(lane_n, 7)
    lane = lane_n - chunk * LANES

    def spread_map(k):
        inside = (lane >= k * p.cpc) & (lane < (k + 1) * p.cpc)
        same = row_i == chunk * p.cpc + lane - k * p.cpc
        return jnp.where(inside & same, 1.0, 0.0).astype(BF)

    for k in range(4, 7):
        loads[k].wait()
    maps = [spread_map(k) for k in range(3)]
    s_in[...] = (dot(sgv[...], maps[0], 0, 0) + dot(suv[...], maps[1], 0, 0)).astype(BF)
    s_back[...] = dot(sdv[...], maps[2], 0, 0).astype(BF)
    s_out_w[...] = (dot(maps[1], sgv[...], 0, 0) + dot(maps[2], suv[...], 0, 0)).astype(BF)

    ids = (
        ep * p.experts + lax.broadcasted_iota(jnp.int32, (p.e_rows, p.tok), 0)
    ).astype(F32)
    before = jnp.where(
        lax.broadcasted_iota(jnp.int32, (p.tok, p.tok), 0)
        < lax.broadcasted_iota(jnp.int32, (p.tok, p.tok), 1),
        1.0,
        0.0,
    ).astype(BF)
    place_in = lax.broadcasted_iota(jnp.int32, (p.slots, p.tok), 0).astype(F32)
    spare = p.rows - p.experts * p.slots

    def route(w):
        sums = [jnp.zeros((p.slots, 1), F32) for _ in range(p.experts)]
        for i in range(p.bpw):
            info = all_meta[order[w * p.bpw + i]]
            chosen = jnp.zeros((p.e_rows, p.tok), F32)
            weight_of = jnp.zeros((p.e_rows, p.tok), F32)
            for k in range(p.picks):
                same = info[k : k + 1, :] == ids
                chosen = jnp.where(same, 1.0, chosen)
                weight_of = jnp.where(
                    same, info[p.picks + k : p.picks + k + 1, :], weight_of
                )
            rank = dot(chosen.astype(BF), before, 1, 0)
            slot = jnp.where(chosen > 0.0, rank + float(p.capacity * i), -1.0)
            for e in range(p.experts):
                hot = place_in == slot[e : e + 1, :]
                oh[w, i, pl.ds(e * p.slots, p.slots), :] = jnp.where(hot, 1.0, 0.0).astype(BF)
                sums[e] = sums[e] + jnp.sum(
                    jnp.where(hot, weight_of[e : e + 1, :], 0.0), axis=1, keepdims=True
                )
            if spare:
                oh[w, i, pl.ds(p.experts * p.slots, spare), :] = jnp.zeros((spare, p.tok), BF)
        for e in range(p.experts):
            rw[w, pl.ds(e * p.slots, p.slots), :] = jnp.broadcast_to(sums[e], (p.slots, LANES))
        if spare:
            rw[w, pl.ds(p.experts * p.slots, spare), :] = jnp.zeros((spare, LANES), F32)

    def pick(w, source):
        total = dot(oh[w, 0], source[order[w * p.bpw]], 1, 0)
        for i in range(1, p.bpw):
            total = total + dot(oh[w, i], source[order[w * p.bpw + i]], 1, 0)
        return total

    def wave_rows(w, source):
        return join([source[order[w * p.bpw + i]] for i in range(p.bpw)], 0)

    def swap_copy(w):
        return remote(full.at[w, 1 - parity], got.at[w], a_s.at[w], a_r.at[w], partner)

    def put(w, e, kind, value):
        q, at = p.strip(e)
        for c in range(nc):
            full[
                w, q // nr, (q % nr) * nc + c, pl.ds(kind * p.rc + at, p.slots), :
            ] = value[:, c * LANES : (c + 1) * LANES]

    def fill(w):
        for i in range(p.bpw):
            arrive(w * p.bpw + i)
        route(w)
        recv_x[w] = pick(w, all_x).astype(BF)
        if w == 0:
            loads[7].wait()
            loads[8].wait()
        for kind, weight in ((0, wg), (1, wu)):
            for e in range(p.experts):
                put(w, e, kind, dot(recv_x[w, pl.ds(e * p.slots, p.slots), :], weight[e], 1, 0))
        recv_dy = pick(w, all_dy)
        weighted[w] = (rw[w][:, :1] * recv_dy).astype(BF)
        narrow_dy = recv_dy.astype(BF)
        if w == 0:
            loads[9].wait()
        for e in range(p.experts):
            put(w, e, 2, dot(narrow_dy[e * p.slots : (e + 1) * p.slots, :], wd[e], 1, 1))
        for s in range(p.experts, p.rows // p.slots):
            for kind in range(3):
                put(w, s, kind, jnp.zeros((p.slots, p.ff), F32))
        s = dot(wave_rows(w, all_x), s_in[...], 1, 0) + dot(
            wave_rows(w, all_dy), s_back[...], 1, 0
        )
        for q in range(2 * nr):
            for c in range(nc):
                full[w, q // nr, (q % nr) * nc + c, pl.ds(3 * p.rc, p.sc), :] = s[
                    q * p.sc : (q + 1) * p.sc, c * LANES : (c + 1) * LANES
                ]
        swap_copy(w).start()

    def scatter_copy(w, d):
        return remote(
            held.at[w, others[d]], landed.at[w, d], b_s.at[w, d], b_r.at[w, d], places[d]
        )

    def scatter(w):
        swap_copy(w).wait_recv()
        for d, j in enumerate(others):
            held[w, j] = (full[w, parity, j] + got[w, j]).astype(BF)
            scatter_copy(w, d).start()

    def gather_copy(w, d, block):
        ref = acts.at[w, block]
        return remote(ref, ref, c_s.at[w, d], c_r.at[w, d], places[d])

    def side_copy(w, d, block):
        ref = acts.at[w, block]
        return remote(ref, ref, d_s.at[w, d], d_r.at[w, d], partner)

    def activate(w):
        out = full[w, parity, mine] + got[w, mine]
        for d in range(half - 1):
            scatter_copy(w, d).wait_recv()
            out = out + landed[w, d].astype(F32)
        gate, up, back = (out[k * p.rc : (k + 1) * p.rc] for k in range(3))
        silu_out, silu_slope = silu_parts(gate)
        hidden = (silu_out * up).astype(BF)
        band = parity * nr + mine // nc
        weight = rw[w, pl.ds(pl.multiple_of(band * p.rc, p.rc), p.rc), :]
        dhidden = weight * back
        acts[w, place, pl.ds(0, p.rc), :] = hidden
        acts[w, place, pl.ds(p.rc, p.rc), :] = (dhidden * up * silu_slope).astype(BF)
        acts[w, place, pl.ds(2 * p.rc, p.rc), :] = (dhidden * silu_out).astype(BF)
        dots = dot(
            jnp.ones((16, LANES), F32), hidden.astype(F32) * back, 1, 1, lax.Precision.HIGHEST
        )
        high = dots.astype(BF).astype(F32)
        mid = (dots - high).astype(BF).astype(F32)
        low = dots - high - mid
        line = lax.broadcasted_iota(jnp.int32, dots.shape, 0)
        pieces = jnp.where(line == 0, high, jnp.where(line == 1, mid, low))
        acts[w, place, pl.ds(3 * p.rc, 16), pl.ds(0, p.rc)] = pieces.astype(BF)
        both = out[3 * p.rc :]
        at = lax.broadcasted_iota(jnp.int32, both.shape, 1)
        s_up = pltpu.roll(both, LANES - p.cpc, 1)
        s_bk = pltpu.roll(both, LANES - 2 * p.cpc, 1)
        s_out, s_slope = silu_parts(both)
        s_dgate = pltpu.roll(s_bk * s_up * s_slope, p.cpc, 1)
        s_dup = pltpu.roll(s_bk * s_out, 2 * p.cpc, 1)
        value = jnp.where(
            at < p.cpc,
            s_out * s_up,
            jnp.where(at < 2 * p.cpc, s_dgate, jnp.where(at < 3 * p.cpc, s_dup, 0.0)),
        )
        acts[w, place, pl.ds(3 * p.rc + 16, p.sc), :] = value.astype(BF)
        for d in range(half - 1):
            gather_copy(w, d, place).start()
        side_copy(w, 0, place).start()

    def origin(d):
        return lax.rem(mine + half - 1 - d, half)

    def forward(w):
        for d in range(half - 1):
            block = parity * half + origin(d)
            gather_copy(w, d, block).wait_recv()
            side_copy(w, 1 + d, block).start()

    def strip_of(w, kind, e):
        q, at = p.strip(e)
        return join(
            [acts[w, p.place(q, c), pl.ds(kind * p.rc + at, p.slots), :] for c in range(nc)], 1
        )

    def shared_rows(w):
        return join(
            [
                join(
                    [
                        acts[w, p.place(q, c), pl.ds(3 * p.rc + 16, p.sc), :]
                        for c in range(nc)
                    ],
                    1,
                )
                for q in range(2 * nr)
            ],
            0,
        )

    def home_copies(b):
        return (
            remote(part.at[b], part_in.at[ep], r_s.at[b, 0], r_r.at[ep, 0], {"ep": b}),
            remote(wpart.at[b], wpart_in.at[ep], r_s.at[b, 1], r_r.at[ep, 1], {"ep": b}),
        )

    def send_home(w):
        side_copy(w, 0, (1 - parity) * half + mine).wait_recv()
        for d in range(half - 1):
            side_copy(w, 1 + d, (1 - parity) * half + origin(d)).wait_recv()
        row_grad = []
        for e in range(p.experts):
            row_grad.append(
                (
                    dot(strip_of(w, 1, e), wg[e], 1, 1) + dot(strip_of(w, 2, e), wu[e], 1, 1)
                ).astype(BF)
            )
        if spare:
            row_grad.append(jnp.zeros((spare, p.narrow), BF))
        row_grad = join(row_grad, 0)
        s_grad = dot(shared_rows(w), s_out_w[...], 1, 0)
        row_e = lax.broadcasted_iota(jnp.int32, (p.e_rows, p.rc), 0)
        row_l = lax.broadcasted_iota(jnp.int32, (p.e_rows, p.rc), 1)
        masked = []
        for q in range(2 * nr):
            line = jnp.zeros((1, p.rc), F32)
            for c in range(nc):
                pieces = acts[w, p.place(q, c), pl.ds(3 * p.rc, 16), pl.ds(0, p.rc)].astype(F32)
                line = line + (pieces[0:1] + pieces[1:2] + pieces[2:3])
            row = row_l + q * p.rc
            inside = (row >= row_e * p.slots) & (row < (row_e + 1) * p.slots)
            masked.append(jnp.where(inside, line, 0.0))
        for i in range(p.bpw):
            b = order[w * p.bpw + i]
            value = dot(oh[w, i], row_grad, 0, 0) + s_grad[i * p.tok : (i + 1) * p.tok, :]

            info = all_meta[b]
            dot_of = jnp.zeros((p.e_rows, p.tok), F32)
            for q in range(2 * nr):
                dot_of = dot_of + dot(
                    masked[q], oh[w, i, pl.ds(q * p.rc, p.rc), :].astype(F32), 1, 0,
                    lax.Precision.HIGHEST,
                )
            for k in range(p.picks):
                wpart[b, pl.ds(k, 1), :] = jnp.sum(
                    jnp.where(info[k : k + 1, :] == ids, dot_of, 0.0), axis=0, keepdims=True
                )
            if w == 0 and i == 0:
                own[...] = value
            else:
                part[b] = value.astype(BF)
                for c in home_copies(b):
                    c.start()

    wpart[...] = jnp.zeros_like(wpart)
    waves = p.waves
    for step in range(waves + 3):
        if step < waves:
            fill(step)
            scatter(step)
        if 1 <= step <= waves:
            activate(step - 1)
        if 2 <= step <= waves + 1:
            forward(step - 2)
        if 3 <= step:
            send_home(step - 3)

    def stacked(strips):
        return join(strips, 0)

    def pile(ref, e):
        return stacked([ref[w, pl.ds(e * p.slots, p.slots), :] for w in range(waves)])

    def pile_acts(kind, e):
        return stacked([strip_of(w, kind, e) for w in range(waves)])

    ts[...] = jnp.zeros_like(ts)
    es[...] = jnp.zeros_like(es)
    for e in range(p.experts):
        down = dot(pile_acts(0, e), pile(weighted, e), 0, 0)
        down_out[e] = down
        ts[pl.ds(e, 1), :] = row_squares(down * down)
    so = stacked([shared_rows(w) for w in range(waves)])
    pair[0] = dot(so, stacked([wave_rows(w, all_x) for w in range(waves)]), 0, 0)
    pair[1] = dot(so, stacked([wave_rows(w, all_dy) for w in range(waves)]), 0, 0)
    for c in range(nc):
        size = min(p.cpc, p.cols - c * p.cpc)
        if size <= 0:
            continue
        to = pl.ds(c * p.cpc, size)
        sd_out[to, :] = pair[0 + 1, pl.ds(c * LANES, size), :]
        sg_out[to, :] = pair[0, pl.ds(c * LANES + p.cpc, size), :]
        su_out[to, :] = pair[0, pl.ds(c * LANES + 2 * p.cpc, size), :]
    sg, su, sd = sg_out[...], su_out[...], sd_out[...]
    es[0:1, :] = jnp.sum(sg * sg, axis=0, keepdims=True)
    es[1:2, :] = jnp.sum(su * su, axis=0, keepdims=True)
    ts[pl.ds(p.experts, 1), pl.ds(0, p.cols)] = row_squares(sd * sd)
    last = []
    for d, q in enumerate(eps):
        last.append(remote(es, es_in.at[d], e_s.at[d], e_r.at[d], {"ep": q}))
    for d, q in enumerate(tps):
        last.append(remote(ts, ts_in.at[d], t_s.at[d], t_r.at[d], {"tp": q}))
    for c in last:
        c.start()
    for e in range(p.experts):
        rows = pile(recv_x, e)
        gate = dot(rows, pile_acts(1, e), 0, 0)
        gate_out[e] = gate
        gate_sq[pl.ds(e, 1), :] = row_squares(gate * gate)
        up = dot(rows, pile_acts(2, e), 0, 0)
        up_out[e] = up
        up_sq[pl.ds(e, 1), :] = row_squares(up * up)

    total = own[...]
    w_total = wpart[ep]
    for b in eps:
        for ref, k in ((part_in, 0), (wpart_in, 1)):
            remote(ref.at[b], ref.at[b], r_s.at[b, k], r_r.at[b, k], {"ep": b}).wait_recv()
        total = total + part_in[b].astype(F32)
        w_total = w_total + wpart_in[b]
    token_out[...] = total.astype(BF)
    weight_out[...] = w_total[: p.picks]
    for c in last:
        c.wait_recv()
    norms = es[...]
    for d in range(n_ep - 1):
        norms = norms + es_in[d]
    sg_sq[...] = norms[0:1]
    su_sq[...] = norms[1:2]
    rows = ts[...]
    for d in range(n_tp - 1):
        rows = rows + ts_in[d]
    down_sq[...] = rows[: p.experts]
    sd_sq[...] = rows[p.experts : p.experts + 1, : p.cols]

    for cond, side, step in ((go_right, 0, 1), (go_left, 1, -1)):

        @pl.when(cond)
        def _(side=side, step=step):
            for k in range(3):
                relay(ep, k, zo.at[side, k], step).wait_send()

    for k in range(1, n_ep):
        b = order[k]

        @pl.when(((b < ep) & go_right) | ((b > ep) & go_left))
        def _(b=b):
            for a in range(3):
                relay(b, a, zs.at[b, a], 0).wait_send()

        for c in home_copies(b):
            c.wait_send()
    for w in range(waves):
        swap_copy(w).wait_send()
        for d in range(half - 1):
            scatter_copy(w, d).wait_send()
            gather_copy(w, d, place).wait_send()
        for d in range(half):
            side_copy(w, d, place).wait_send()
    for c in last:
        c.wait_send()


def copy_kernel(count, *refs):
    srcs, dsts, sem = refs[:count], refs[count : 2 * count], refs[2 * count]
    copies = [
        pltpu.make_async_copy(srcs[k], dsts[k], sem.at[k]) for k in range(count)
    ]
    for c in copies:
        c.start()
    for c in copies:
        c.wait()


def per_device(
    n_ep, n_tp,
    tokens, cotangent, routes, gate_weights,
    expert_gate, expert_up, expert_down,
    shared_gate, shared_up, shared_down,
):
    dma = pltpu.SemaphoreType.DMA
    vm = pltpu.VMEM
    tok, narrow = tokens.shape
    picks = routes.shape[1]
    experts, _, ff = expert_gate.shape
    p = Plan(n_ep, n_tp, tok, picks, narrow, experts, ff, shared_gate.shape[1])
    half, waves = p.half, p.waves
    meta_rows = up_to(2 * picks, 8)
    ts_rows = up_to(experts + 1, 8)
    wide = p.nc * LANES
    outs = [
        ((tok, narrow), BF), ((picks, tok), F32),
        ((experts, narrow, ff), F32), ((experts, narrow, ff), F32), ((experts, ff, narrow), F32),
        ((p.cols, narrow), F32), ((p.cols, narrow), F32), ((p.cols, narrow), F32),
        ((experts, narrow), F32), ((experts, narrow), F32), ((experts, ff), F32),
        ((1, narrow), F32), ((1, narrow), F32), ((1, p.cols), F32),
    ]
    out_shape = [jax.ShapeDtypeStruct(s, t) for s, t in outs]
    out_bytes = sum(
        up_to(s[-2], 8) * up_to(s[-1], LANES) * (s[0] if len(s) == 3 else 1) * jnp.dtype(t).itemsize
        for s, t in outs
    )
    grant = (VMEM_BYTES - out_bytes) // 2**18 * 2**18 - ROOM
    results = pl.pallas_call(
        functools.partial(main_kernel, p),
        out_shape=out_shape,
        in_specs=[HBM] * 10,
        out_specs=[VMEM] * len(outs),
        scratch_shapes=[
            vm(expert_gate.shape, BF), vm(expert_up.shape, BF), vm(expert_down.shape, BF),
            vm((p.cols, narrow), BF), vm((p.cols, narrow), BF), vm((p.cols, narrow), BF),
            vm((picks, tok), jnp.int32), vm((picks, tok), F32),
            vm((n_ep, tok, narrow), BF), vm((n_ep, tok, narrow), BF),
            vm((n_ep, meta_rows, tok), F32),
            vm((narrow, wide), BF), vm((narrow, wide), BF), vm((wide, narrow), BF),
            vm((waves, p.bpw, p.rows, tok), BF),
            vm((waves, p.rows, narrow), BF), vm((waves, p.rows, narrow), BF),
            vm((waves, p.rows, LANES), F32),
            vm((waves, 2, half, p.slab, LANES), F32),
            vm((waves, half, p.slab, LANES), F32),
            vm((waves, half, p.slab, LANES), BF),
            vm((waves, half - 1, p.slab, LANES), BF),
            vm((waves, n_tp, p.out_slab, LANES), BF),
            vm((2, wide, narrow), F32),
            vm((n_ep, tok, narrow), BF), vm((n_ep, tok, narrow), BF), vm((tok, narrow), F32),
            vm((n_ep, 8, tok), F32), vm((n_ep, 8, tok), F32),
            vm((ts_rows, ff), F32), vm((n_tp - 1, ts_rows, ff), F32),
            vm((8, narrow), F32), vm((n_ep - 1, 8, narrow), F32),
            dma((10,)), dma((2, 3)), dma((n_ep, 3)), dma((n_ep, 3)),
            dma((waves,)), dma((waves,)),
            dma((waves, half - 1)), dma((waves, half - 1)),
            dma((waves, half - 1)), dma((waves, half - 1)),
            dma((waves, half)), dma((waves, half)),
            dma((n_ep, 2)), dma((n_ep, 2)),
            dma((n_ep - 1,)), dma((n_ep - 1,)), dma((n_tp - 1,)), dma((n_tp - 1,)),
        ],
        compiler_params=pltpu.CompilerParams(
            collective_id=0, has_side_effects=True, vmem_limit_bytes=grant
        ),
    )(
        *[
            pltpu.with_memory_space_constraint(a, pltpu.HBM)
            for a in (
                tokens, cotangent, routes.T, gate_weights.T,
                expert_gate, expert_up, expert_down,
                shared_gate.T, shared_up.T, shared_down,
            )
        ]
    )
    count = len(outs)
    (
        token_grad, weight_grad, gate, up, down, sg, su, sd,
        gate_sq, up_sq, down_sq, sg_sq, su_sq, sd_sq,
    ) = pl.pallas_call(
        functools.partial(copy_kernel, count),
        out_shape=out_shape,
        in_specs=[VMEM] * count,
        out_specs=[HBM] * count,
        scratch_shapes=[dma((count,))],
        compiler_params=pltpu.CompilerParams(vmem_limit_bytes=20 * 1024 * 1024),
    )(*results)
    return (
        token_grad, weight_grad.T, gate, up, down, sg.T, su.T, sd,
        gate_sq, up_sq, down_sq, sg_sq[0], su_sq[0], sd_sq[0],
    )


def solution(mesh):
    n_ep, n_tp = mesh.shape["ep"], mesh.shape["tp"]
    return jax.shard_map(
        functools.partial(per_device, n_ep, n_tp),
        mesh=mesh,
        in_specs=(
            P("ep", "tp"),
            P("ep", "tp"),
            P("ep", None),
            P("ep", None),
            P("ep", "tp", None),
            P("ep", "tp", None),
            P("ep", None, "tp"),
            P("tp", None),
            P("tp", None),
            P(None, "tp"),
        ),
        out_specs=(
            P("ep", "tp"),
            P("ep", None),
            P("ep", "tp", None),
            P("ep", "tp", None),
            P("ep", None, "tp"),
            P("tp", "ep"),
            P("tp", "ep"),
            P("ep", "tp"),
            P("ep", "tp"),
            P("ep", "tp"),
            P("ep", None),
            P("tp"),
            P("tp"),
            P("ep"),
        ),
        check_vma=False,
    )
```

time: 79.7 us -> 53.8 us (0.68)
  local copies, waits for them, and re-layouts: 10.7 us -> 0 us
  Pallas kernels: 58.9 us -> 53 us
  other arithmetic: 4.69 us -> 0 us
  starting transfers between devices: 4.17 us -> 0 us
    unnamed x27 -> x0, local copies, waits for them, and re-layouts: 6.41 us -> none
    pallas_call x3 -> x2, Pallas kernels: 58.9 us -> 53 us  [the longest x1 49.1 us: per_device(): pl.pallas_call(functools.partial(main_kernel, p), out_shape=out_shape, in...]
    ppermute x3 -> x0, starting transfers between devices: 4.17 us -> none  [per_device(): lax.ppermute(lax.dynamic_index_in_dim(token_part, lax.rem(ep + d, n_ep),...]
    convert_element_type x2 -> x0, other arithmetic: 2.21 us -> none  [the longest x1 1.69 us: per_device(): token_grad = token_grad.astype(BF)]
    slice x5 -> x0, local copies, waits for them, and re-layouts: 1.92 us -> none  [the longest x1 0.77 us: per_device(): dots[:, 0, :].reshape(rows)[:used].reshape(1, experts, per_expert, 1)]
    reduce_sum x2 -> x0, other arithmetic: 1.06 us -> none  [the longest x1 0.75 us: per_device(): weight_part = jnp.sum(jnp.where(match, dot_of[:, None], 0.0), axis=2)]
    dynamic_slice x2 -> x0, local copies, waits for them, and re-layouts: 0.94 us -> none  [the longest x1 0.93 us: per_device(): su = lax.dynamic_slice_in_dim(shared_up.T, ep * cols, cols, 0)]
  transfers between devices with their start and end apart: 3 -> 0, of which waited for: 0 -> 0; matrix products, arithmetic and copies ran while one was open for 5% -> 0% of each run, Pallas kernels for 18% -> 0%
where the time goes in v1:
time: 53.8 us; the launch traced here: 53.7 us
  Pallas kernels  53 us (99%)
  between operations  0.66 us (1%)
    pallas_call x1, Pallas kernels, per_device(): pl.pallas_call(functools.partial(main_kernel, p), out_shape=out_shape, in...  49.1 us
    pallas_call x1, Pallas kernels, per_device(): pl.pallas_call(functools.partial(copy_kernel, count), out_shape=out_shape...  3.95 us

profile of v1, /device:TPU:0, one launch (start us, length us, event | category | flops | bytes accessed | tf_op | source)
XLA Modules:
  0.0 53.7 jit_solution(6220898286665415603)
XLA Ops:
  0.7 49.1 %shard_map.209 = (bf16[160,256]{1,0:T(8,128)(2,1)S(1)}, f32[2,160]{1,0:T(2,128)S(1)}, f32[6,256,512]{2,1,0:T(8,128)S(1)}, f32[6,256,512]{2,1,0:T(8,128)S(1)}, f3...) custom-call(bf16[160,256]{1,0:T(8,128)(2,1)} %x.1, ...), custom_call_target="tpu_custom_call" | custom-call | tf_op jit(solution)/shard_map/pallas_call | solution.py:587
  49.7 3.9 %shard_map.210 = (bf16[160,256]{1,0:T(8,128)(2,1)}, f32[2,160]{1,0:T(2,128)}, f32[6,256,512]{2,1,0:T(8,128)}, f32[6,256,512]{2,1,0:T(8,128)}, f32[6,512,256]{2,1...) custom-call(bf16[160,256]{1,0:T(8,128)(2,1)S(1)} %get-tuple-element., ...), custom_call_target="tpu_custom_call" | custom-call | tf_op jit(solution)/shard_map/pallas_call | solution.py:637

commit v2 on v1

--- a/solution.py
+++ b/solution.py
@@ -125,7 +125,12 @@
     places = [{"tp": 2 * j + parity} for j in others]
     eps = [lax.rem(ep + d, n_ep) for d in range(1, n_ep)]
     tps = [lax.rem(me + d, n_tp) for d in range(1, n_tp)]
-    order = [nearest(ep, n_ep, k) for k in range(n_ep)]
+    arrival = [nearest(ep, n_ep, k) for k in range(n_ep)]
+    order = list(arrival)
+    if n_ep == 4:
+        middle = (ep == 1) | (ep == 2)
+        order[2] = jnp.where(middle, arrival[3], arrival[2])
+        order[3] = jnp.where(middle, arrival[2], arrival[3])
     place = parity * half + mine
 
     barrier = pltpu.get_barrier_semaphore()
@@ -154,7 +159,6 @@
     )
     loads[0].wait()
     loads[1].wait()
-    pl.semaphore_wait(barrier, n_ep + n_tp - 2)
 
     blocks = (all_meta, all_x, all_dy)
 
@@ -164,27 +168,46 @@
         )
 
     go_right, go_left = ep < n_ep - 1, ep > 0
-    for cond, side, step in ((go_right, 0, 1), (go_left, 1, -1)):
-
-        @pl.when(cond)
-        def _(side=side, step=step):
-            for k in range(3):
-                relay(ep, k, zo.at[side, k], step).start()
-
-    def arrive(k):
-        b = order[k]
-        if k == 0:
-            return
-        for a in range(3):
+
+    def send_own():
+        for cond, side, step in ((go_right, 0, 1), (go_left, 1, -1)):
+
+            @pl.when(cond)
+            def _(side=side, step=step):
+                for k in range(3):
+                    relay(ep, k, zo.at[side, k], step).start()
+
+    def arrive(k, arrays):
+        b = arrival[k]
+        for a in arrays:
             relay(b, a, zs.at[b, a], 0).wait_recv()
 
             @pl.when((b < ep) & go_right)
-            def _():
+            def _(a=a):
                 relay(b, a, zs.at[b, a], 1).start()
 
             @pl.when((b > ep) & go_left)
-            def _():
+            def _(a=a):
                 relay(b, a, zs.at[b, a], -1).start()
+
+    reach = 2 * jnp.minimum(ep, n_ep - 1 - ep)
+
+    def take(j, arrays):
+        for k in range(max(j, 1), min(j + 3, n_ep)):
+            early = k - 1 if k % 2 else max(1, k - 2)
+            if k == 1:
+                if j == 1:
+                    arrive(k, arrays)
+            elif j == early or j == k:
+                inside = reach >= k - k % 2
+
+                @pl.when(inside if j == early else jnp.logical_not(inside))
+                def _(k=k):
+                    arrive(k, arrays)
+
+    def take_wave(w, arrays):
+        for i in range(p.bpw):
+            take(w * p.bpw + i, arrays)
 
     lane_n = lax.broadcasted_iota(jnp.int32, (p.cols, nc * LANES), 1)
     row_i = lax.broadcasted_iota(jnp.int32, (p.cols, nc * LANES), 0)
@@ -262,16 +285,18 @@
             ] = value[:, c * LANES : (c + 1) * LANES]
 
     def fill(w):
-        for i in range(p.bpw):
-            arrive(w * p.bpw + i)
-        route(w)
-        recv_x[w] = pick(w, all_x).astype(BF)
+        if w == 0 and p.bpw > 1:
+            take_wave(0, (0, 1))
+        if w > 0 or p.bpw > 1:
+            route(w)
+            recv_x[w] = pick(w, all_x).astype(BF)
         if w == 0:
             loads[7].wait()
             loads[8].wait()
         for kind, weight in ((0, wg), (1, wu)):
             for e in range(p.experts):
                 put(w, e, kind, dot(recv_x[w, pl.ds(e * p.slots, p.slots), :], weight[e], 1, 0))
+        take_wave(w, (2,))
         recv_dy = pick(w, all_dy)
         weighted[w] = (rw[w][:, :1] * recv_dy).astype(BF)
         narrow_dy = recv_dy.astype(BF)
@@ -437,16 +462,32 @@
 
     wpart[...] = jnp.zeros_like(wpart)
     waves = p.waves
-    for step in range(waves + 3):
-        if step < waves:
-            fill(step)
-            scatter(step)
-        if 1 <= step <= waves:
+    if p.bpw == 1:
+        route(0)
+        recv_x[0] = pick(0, all_x).astype(BF)
+    pl.semaphore_wait(barrier, n_ep + n_tp - 2)
+    send_own()
+    for step in range(waves):
+        fill(step)
+        scatter(step)
+        if step + 1 < waves:
+            take_wave(step + 1, (0, 1))
+        if step >= 3:
+            forward(step - 3)
+        if step >= 1:
             activate(step - 1)
-        if 2 <= step <= waves + 1:
-            forward(step - 2)
-        if 3 <= step:
-            send_home(step - 3)
+        if step >= 4:
+            send_home(step - 4)
+    late = max(0, waves - 3)
+    if waves > 2:
+        forward(late)
+        for w in range(max(0, waves - 4), late + 1):
+            send_home(w)
+        late = late + 1
+    activate(waves - 1)
+    for w in range(late, waves):
+        forward(w)
+        send_home(w)
 
     def stacked(strips):
         return join(strips, 0)

time: 53.8 us -> 47.2 us (0.88)
  Pallas kernels: 53 us -> 46.4 us
    pallas_call x1, Pallas kernels: 49.1 us -> 42.5 us  [per_device(): pl.pallas_call(functools.partial(main_kernel, p), out_shape=out_shape, in...]
where the time goes in v2:
time: 47.2 us; the launch traced here: 47.1 us
  Pallas kernels  46.4 us (98%)
  between operations  0.66 us (1%)
    pallas_call x1, Pallas kernels, per_device(): pl.pallas_call(functools.partial(main_kernel, p), out_shape=out_shape, in...  42.5 us
    pallas_call x1, Pallas kernels, per_device(): pl.pallas_call(functools.partial(copy_kernel, count), out_shape=out_shape...  3.95 us

profile of v2, /device:TPU:0, one launch (start us, length us, event | category | flops | bytes accessed | tf_op | source)
XLA Modules:
  0.0 47.1 jit_solution(18006033701060903635)
XLA Ops:
  0.7 42.5 %shard_map.209 = (bf16[160,256]{1,0:T(8,128)(2,1)S(1)}, f32[2,160]{1,0:T(2,128)S(1)}, f32[6,256,512]{2,1,0:T(8,128)S(1)}, f32[6,256,512]{2,1,0:T(8,128)S(1)}, f3...) custom-call(bf16[160,256]{1,0:T(8,128)(2,1)} %x.1, ...), custom_call_target="tpu_custom_call" | custom-call | tf_op jit(solution)/shard_map/pallas_call | solution.py:628
  43.1 3.9 %shard_map.210 = (bf16[160,256]{1,0:T(8,128)(2,1)}, f32[2,160]{1,0:T(2,128)}, f32[6,256,512]{2,1,0:T(8,128)}, f32[6,256,512]{2,1,0:T(8,128)}, f32[6,512,256]{2,1...) custom-call(bf16[160,256]{1,0:T(8,128)(2,1)S(1)} %get-tuple-element., ...), custom_call_target="tpu_custom_call" | custom-call | tf_op jit(solution)/shard_map/pallas_call | solution.py:678

commit v3 on v2

--- a/solution.py
+++ b/solution.py
@@ -92,7 +92,9 @@
         self.cols = shared // n_ep
         self.cpc = -(-self.cols // self.nc)
         self.slab = 3 * self.rc + self.sc
-        self.out_slab = self.slab + 16
+        self.shared_at = 2 * self.rc + 16
+        self.first = self.shared_at + self.sc
+        self.out_slab = self.first + self.rc
         self.e_rows = up_to(experts, 8)
         assert self.half % self.nc == 0 and self.nr > 0 and self.rc <= LANES
         assert self.sc % 16 == 0 and 3 * self.cpc <= LANES
@@ -115,13 +117,21 @@
     full, got, held, landed, acts, pair, part, part_in, own, wpart, wpart_in,
     ts, ts_in, es, es_in,
     ld, zo, zs, zr, a_s, a_r, b_s, b_r, c_s, c_r, d_s, d_r, r_s, r_r, e_s, e_r, t_s, t_r,
+    h_s, h_r,
 ):
     n_ep, n_tp, half, nc, nr = p.n_ep, p.n_tp, p.half, p.nc, p.nr
     ep, me = lax.axis_index("ep"), lax.axis_index("tp")
     parity = lax.rem(me, 2)
     mine = me // 2
     partner = {"tp": me + 1 - 2 * parity}
-    others = [lax.rem(mine + d, half) for d in range(1, half)]
+    if half == 4:
+        flip_x = mine + 1 - 2 * lax.rem(mine, 2)
+        flip_y = mine + 2 - 4 * (mine // 2)
+        others = [3 - mine, flip_y, flip_x]
+        origins = others
+    else:
+        others = [lax.rem(mine + d, half) for d in range(1, half)]
+        origins = [lax.rem(mine + half - d, half) for d in range(1, half)]
     places = [{"tp": 2 * j + parity} for j in others]
     eps = [lax.rem(ep + d, n_ep) for d in range(1, n_ep)]
     tps = [lax.rem(me + d, n_tp) for d in range(1, n_tp)]
@@ -329,12 +339,20 @@
             scatter_copy(w, d).start()
 
     def gather_copy(w, d, block):
-        ref = acts.at[w, block]
+        ref = acts.at[w, block, pl.ds(0, p.first)]
         return remote(ref, ref, c_s.at[w, d], c_r.at[w, d], places[d])
 
     def side_copy(w, d, block):
-        ref = acts.at[w, block]
+        ref = acts.at[w, block, pl.ds(0, p.first)]
         return remote(ref, ref, d_s.at[w, d], d_r.at[w, d], partner)
+
+    def hidden_copy(d, block):
+        ref = acts.at[:, block, pl.ds(p.first, p.rc)]
+        return remote(ref, ref, h_s.at[d], h_r.at[d], places[d])
+
+    def hidden_side(d, block):
+        ref = acts.at[:, block, pl.ds(p.first, p.rc)]
+        return remote(ref, ref, h_s.at[half + d], h_r.at[half + d], partner)
 
     def activate(w):
         out = full[w, parity, mine] + got[w, mine]
@@ -347,9 +365,9 @@
         band = parity * nr + mine // nc
         weight = rw[w, pl.ds(pl.multiple_of(band * p.rc, p.rc), p.rc), :]
         dhidden = weight * back
-        acts[w, place, pl.ds(0, p.rc), :] = hidden
-        acts[w, place, pl.ds(p.rc, p.rc), :] = (dhidden * up * silu_slope).astype(BF)
-        acts[w, place, pl.ds(2 * p.rc, p.rc), :] = (dhidden * silu_out).astype(BF)
+        acts[w, place, pl.ds(0, p.rc), :] = (dhidden * up * silu_slope).astype(BF)
+        acts[w, place, pl.ds(p.rc, p.rc), :] = (dhidden * silu_out).astype(BF)
+        acts[w, place, pl.ds(p.first, p.rc), :] = hidden
         dots = dot(
             jnp.ones((16, LANES), F32), hidden.astype(F32) * back, 1, 1, lax.Precision.HIGHEST
         )
@@ -358,7 +376,7 @@
         low = dots - high - mid
         line = lax.broadcasted_iota(jnp.int32, dots.shape, 0)
         pieces = jnp.where(line == 0, high, jnp.where(line == 1, mid, low))
-        acts[w, place, pl.ds(3 * p.rc, 16), pl.ds(0, p.rc)] = pieces.astype(BF)
+        acts[w, place, pl.ds(2 * p.rc, 16), pl.ds(0, p.rc)] = pieces.astype(BF)
         both = out[3 * p.rc :]
         at = lax.broadcasted_iota(jnp.int32, both.shape, 1)
         s_up = pltpu.roll(both, LANES - p.cpc, 1)
@@ -371,32 +389,28 @@
             s_out * s_up,
             jnp.where(at < 2 * p.cpc, s_dgate, jnp.where(at < 3 * p.cpc, s_dup, 0.0)),
         )
-        acts[w, place, pl.ds(3 * p.rc + 16, p.sc), :] = value.astype(BF)
+        acts[w, place, pl.ds(p.shared_at, p.sc), :] = value.astype(BF)
         for d in range(half - 1):
             gather_copy(w, d, place).start()
         side_copy(w, 0, place).start()
 
-    def origin(d):
-        return lax.rem(mine + half - 1 - d, half)
-
     def forward(w):
         for d in range(half - 1):
-            block = parity * half + origin(d)
+            block = parity * half + origins[d]
             gather_copy(w, d, block).wait_recv()
             side_copy(w, 1 + d, block).start()
 
     def strip_of(w, kind, e):
         q, at = p.strip(e)
-        return join(
-            [acts[w, p.place(q, c), pl.ds(kind * p.rc + at, p.slots), :] for c in range(nc)], 1
-        )
+        at = at + (p.first if kind == 0 else (kind - 1) * p.rc)
+        return join([acts[w, p.place(q, c), pl.ds(at, p.slots), :] for c in range(nc)], 1)
 
     def shared_rows(w):
         return join(
             [
                 join(
                     [
-                        acts[w, p.place(q, c), pl.ds(3 * p.rc + 16, p.sc), :]
+                        acts[w, p.place(q, c), pl.ds(p.shared_at, p.sc), :]
                         for c in range(nc)
                     ],
                     1,
@@ -415,7 +429,7 @@
     def send_home(w):
         side_copy(w, 0, (1 - parity) * half + mine).wait_recv()
         for d in range(half - 1):
-            side_copy(w, 1 + d, (1 - parity) * half + origin(d)).wait_recv()
+            side_copy(w, 1 + d, (1 - parity) * half + origins[d]).wait_recv()
         row_grad = []
         for e in range(p.experts):
             row_grad.append(
@@ -433,7 +447,7 @@
         for q in range(2 * nr):
             line = jnp.zeros((1, p.rc), F32)
             for c in range(nc):
-                pieces = acts[w, p.place(q, c), pl.ds(3 * p.rc, 16), pl.ds(0, p.rc)].astype(F32)
+                pieces = acts[w, p.place(q, c), pl.ds(2 * p.rc, 16), pl.ds(0, p.rc)].astype(F32)
                 line = line + (pieces[0:1] + pieces[1:2] + pieces[2:3])
             row = row_l + q * p.rc
             inside = (row >= row_e * p.slots) & (row < (row_e + 1) * p.slots)
@@ -485,9 +499,16 @@
             send_home(w)
         late = late + 1
     activate(waves - 1)
+    for d in range(half - 1):
+        hidden_copy(d, place).start()
+    hidden_side(0, place).start()
     for w in range(late, waves):
         forward(w)
         send_home(w)
+    for d in range(half - 1):
+        block = parity * half + origins[d]
+        hidden_copy(d, block).wait_recv()
+        hidden_side(1 + d, block).start()
 
     def stacked(strips):
         return join(strips, 0)
@@ -500,10 +521,6 @@
 
     ts[...] = jnp.zeros_like(ts)
     es[...] = jnp.zeros_like(es)
-    for e in range(p.experts):
-        down = dot(pile_acts(0, e), pile(weighted, e), 0, 0)
-        down_out[e] = down
-        ts[pl.ds(e, 1), :] = row_squares(down * down)
     so = stacked([shared_rows(w) for w in range(waves)])
     pair[0] = dot(so, stacked([wave_rows(w, all_x) for w in range(waves)]), 0, 0)
     pair[1] = dot(so, stacked([wave_rows(w, all_dy) for w in range(waves)]), 0, 0)
@@ -518,15 +535,13 @@
     sg, su, sd = sg_out[...], su_out[...], sd_out[...]
     es[0:1, :] = jnp.sum(sg * sg, axis=0, keepdims=True)
     es[1:2, :] = jnp.sum(su * su, axis=0, keepdims=True)
-    ts[pl.ds(p.experts, 1), pl.ds(0, p.cols)] = row_squares(sd * sd)
     last = []
     for d, q in enumerate(eps):
         last.append(remote(es, es_in.at[d], e_s.at[d], e_r.at[d], {"ep": q}))
-    for d, q in enumerate(tps):
-        last.append(remote(ts, ts_in.at[d], t_s.at[d], t_r.at[d], {"tp": q}))
-    for c in last:
-        c.start()
-    for e in range(p.experts):
+        last[-1].start()
+    ts[pl.ds(p.experts, 1), pl.ds(0, p.cols)] = row_squares(sd * sd)
+
+    def gate_up(e):
         rows = pile(recv_x, e)
         gate = dot(rows, pile_acts(1, e), 0, 0)
         gate_out[e] = gate
@@ -534,6 +549,21 @@
         up = dot(rows, pile_acts(2, e), 0, 0)
         up_out[e] = up
         up_sq[pl.ds(e, 1), :] = row_squares(up * up)
+
+    for e in range(p.experts // 3):
+        gate_up(e)
+    hidden_side(0, (1 - parity) * half + mine).wait_recv()
+    for d in range(half - 1):
+        hidden_side(1 + d, (1 - parity) * half + origins[d]).wait_recv()
+    for e in range(p.experts):
+        down = dot(pile_acts(0, e), pile(weighted, e), 0, 0)
+        down_out[e] = down
+        ts[pl.ds(e, 1), :] = row_squares(down * down)
+    for d, q in enumerate(tps):
+        last.append(remote(ts, ts_in.at[d], t_s.at[d], t_r.at[d], {"tp": q}))
+        last[-1].start()
+    for e in range(p.experts // 3, p.experts):
+        gate_up(e)
 
     total = own[...]
     w_total = wpart[ep]
@@ -581,6 +611,10 @@
             gather_copy(w, d, place).wait_send()
         for d in range(half):
             side_copy(w, d, place).wait_send()
+    for d in range(half - 1):
+        hidden_copy(d, place).wait_send()
+    for d in range(half):
+        hidden_side(d, place).wait_send()
     for c in last:
         c.wait_send()
 
@@ -657,6 +691,7 @@
             dma((waves, half)), dma((waves, half)),
             dma((n_ep, 2)), dma((n_ep, 2)),
             dma((n_ep - 1,)), dma((n_ep - 1,)), dma((n_tp - 1,)), dma((n_tp - 1,)),
+            dma((n_tp,)), dma((n_tp,)),
         ],
         compiler_params=pltpu.CompilerParams(
             collective_id=0, has_side_effects=True, vmem_limit_bytes=grant

time: 47.2 us -> 46.2 us (0.979)
  Pallas kernels: 46.4 us -> 45.3 us
    pallas_call x1, Pallas kernels: 42.5 us -> 41.4 us  [per_device(): pl.pallas_call(functools.partial(main_kernel, p), out_shape=out_shape, in...]
where the time goes in v3:
time: 46.2 us; the launch traced here: 46 us
  Pallas kernels  45.3 us (98%)
  between operations  0.66 us (1%)
    pallas_call x1, Pallas kernels, per_device(): pl.pallas_call(functools.partial(main_kernel, p), out_shape=out_shape, in...  41.4 us
    pallas_call x1, Pallas kernels, per_device(): pl.pallas_call(functools.partial(copy_kernel, count), out_shape=out_shape...  3.95 us

profile of v3, /device:TPU:0, one launch (start us, length us, event | category | flops | bytes accessed | tf_op | source)
XLA Modules:
  0.0 46.0 jit_solution(16187810553674660167)
XLA Ops:
  0.7 41.4 %shard_map.209 = (bf16[160,256]{1,0:T(8,128)(2,1)S(1)}, f32[2,160]{1,0:T(2,128)S(1)}, f32[6,256,512]{2,1,0:T(8,128)S(1)}, f32[6,256,512]{2,1,0:T(8,128)S(1)}, f3...) custom-call(bf16[160,256]{1,0:T(8,128)(2,1)} %x.1, ...), custom_call_target="tpu_custom_call" | custom-call | tf_op jit(solution)/shard_map/pallas_call | solution.py:662
  42.1 3.9 %shard_map.210 = (bf16[160,256]{1,0:T(8,128)(2,1)}, f32[2,160]{1,0:T(2,128)}, f32[6,256,512]{2,1,0:T(8,128)}, f32[6,256,512]{2,1,0:T(8,128)}, f32[6,512,256]{2,1...) custom-call(bf16[160,256]{1,0:T(8,128)(2,1)S(1)} %get-tuple-element., ...), custom_call_target="tpu_custom_call" | custom-call | tf_op jit(solution)/shard_map/pallas_call | solution.py:713
